TPU v7x, 32 devices: a whole 2x2x4 slice. The times are simulated.
32 devices in a mesh: ra: 4 (over z), cb: 8 (over y, x, core).
Axes of the slice: x: 2, y: 2, z: 4, core: 2. Of those that a mesh axis runs over, the one named last changes fastest.
Arguments:
- tokens: bfloat16 [2, 128, 3072], P(None, None, 'ra'), may hold values from -70 to 70
- norm_gain: float32 [2, 3072], P(None, 'ra'), may hold values from 0.1 to 1.9
- gate_weight: float32 [2, 3072, 8448], P(None, 'ra', 'cb'), may hold values from -0.109375 to 0.109375
- gate_scale: float32 [2, 8448], P(None, 'cb'), may hold values from 0.5 to 2
- up_weight: float32 [2, 3072, 8448], P(None, 'ra', 'cb'), may hold values from -0.109375 to 0.109375
- up_scale: float32 [2, 8448], P(None, 'cb'), may hold values from 0.5 to 2
- conv_weight: float32 [2, 3, 8448], P(None, None, 'cb'), may hold values from -3.5 to 3.5
- conv_bias: float32 [2, 8448], P(None, 'cb'), may hold values from -3 to 3
- down_weight: float32 [2, 8448, 3072], P(None, 'cb', 'ra'), may hold values from -0.0625 to 0.0625
- down_scale: float32 [2, 3072], P(None, 'ra'), may hold values from 0.5 to 2
Outputs:
- layer_output: bfloat16 [2, 128, 3072], P(None, None, 'ra')
All inputs are finite; a program needn't handle non-finite values.
Results may differ from a plain program's by a relative error of at most 0.014.
Values may be sent and summed in bfloat16 or wider, within the bound.
A program may use at most 64 MiB of HBM per device.

v0:
```python
import jax
import jax.numpy as jnp
from jax import lax
from jax.sharding import PartitionSpec as P

WIDTH = 3072
eps = 1e-06
residual_keep = 0.5


def causal_mix(gate_seq, conv_taps, conv_shift):
    count = conv_taps.shape[0]
    length = gate_seq.shape[1]
    padded = jnp.pad(gate_seq, ((0, 0), (count - 1, 0), (0, 0)))
    running = jnp.zeros_like(gate_seq) + conv_shift[None, None, :]
    for offset in range(count):
        running = (
            running + conv_taps[offset][None, None, :] * padded[:, offset : offset + length, :]
        )
    return running


def sublayer(current, norm_g, gate_w, gate_s, up_w, up_s, conv_taps, conv_shift, down_w, down_s):
    sequences, length, local_width = current.shape
    row_count = sequences * length
    values = current.astype(jnp.float32).reshape(row_count, local_width)
    squares = jnp.sum(values * values, axis=1)
    scaled = (values * norm_g[None, :]).astype(jnp.bfloat16)
    gate_part = jnp.dot(scaled, gate_w.astype(jnp.bfloat16), preferred_element_type=jnp.float32)
    up_part = jnp.dot(scaled, up_w.astype(jnp.bfloat16), preferred_element_type=jnp.float32)
    gate_sum, up_sum = (
        lax.psum_scatter(gate_part, "ra", scatter_dimension=1, tiled=True),
        lax.psum_scatter(up_part, "ra", scatter_dimension=1, tiled=True),
    )
    square_sum = lax.psum(squares, "ra")
    share_cols = gate_sum.shape[1]
    col_start = lax.axis_index("ra") * share_cols
    col_gate = lax.dynamic_slice_in_dim(gate_s, col_start, share_cols, 0)
    col_up = lax.dynamic_slice_in_dim(up_s, col_start, share_cols, 0)
    used_taps = lax.dynamic_slice_in_dim(conv_taps, col_start, share_cols, 1)
    used_shift = lax.dynamic_slice_in_dim(conv_shift, col_start, share_cols, 0)
    inverse_rms = lax.rsqrt(square_sum / WIDTH + eps)[:, None]
    gate_sum = gate_sum * inverse_rms * col_gate[None, :]
    up_sum = up_sum * inverse_rms * col_up[None, :]
    units = gate_sum.shape[1]
    conv_out = causal_mix(gate_sum.reshape(sequences, length, units), used_taps, used_shift)
    hidden_act = (jax.nn.silu(conv_out) * up_sum.reshape(sequences, length, units)).astype(
        jnp.bfloat16
    )
    hidden_act = hidden_act.reshape(row_count, units)
    hidden_act = lax.all_gather(hidden_act, "ra", axis=1, tiled=True)
    down_part = jnp.dot(hidden_act, down_w.astype(jnp.bfloat16), preferred_element_type=jnp.float32)
    down_sum = lax.psum(down_part, "cb")
    branch = down_sum * down_s[None, :]
    return (
        (residual_keep * values + branch)
        .astype(jnp.bfloat16)
        .reshape(sequences, length, local_width)
    )


def shards(
    tokens,
    norm_gain,
    gate_weight,
    gate_scale,
    up_weight,
    up_scale,
    conv_weight,
    conv_bias,
    down_weight,
    down_scale,
):
    current = tokens
    for layer_index in range(2):
        current = sublayer(
            current,
            norm_gain[layer_index],
            gate_weight[layer_index],
            gate_scale[layer_index],
            up_weight[layer_index],
            up_scale[layer_index],
            conv_weight[layer_index],
            conv_bias[layer_index],
            down_weight[layer_index],
            down_scale[layer_index],
        )
    return current


def solution(mesh):
    in_specs = (
        P(None, None, "ra"),
        P(None, "ra"),
        P(None, "ra", "cb"),
        P(None, "cb"),
        P(None, "ra", "cb"),
        P(None, "cb"),
        P(None, None, "cb"),
        P(None, "cb"),
        P(None, "cb", "ra"),
        P(None, "ra"),
    )
    out_specs = P(None, None, "ra")
    return jax.shard_map(shards, mesh=mesh, in_specs=in_specs, out_specs=out_specs, check_vma=False)
```

profile of v0, /device:TPU:0, one launch (start us, length us, event | category | flops | bytes accessed | tf_op | source)
XLA Modules:
  0.0 304.9 jit_solution(4028201805180705221)
XLA Ops:
  6.5 1.4 slice_reduce_fusion.1
  7.9 3.2 %convert.12 = bf16[2,768,1056]{1,2,0:T(8,128)(2,1)S(1)} convert(f32[2,768,1056]{1,2,0:T(8,128)} %param.12) | non-fusion elementwise | flops 1622016 | bytes 9732096 | tf_op jit(solution)/shard_map/convert.5
  11.1 1.2 convert_multiply_fusion.5
  12.4 0.7 copy-done
  13.1 1.6 fusion.5
  14.7 0.0 reduce-scatter.5.cloned.1.call-update
  14.7 0.0 reduce-scatter.7.cloned.1.call-start
  14.8 3.2 %convert.13 = bf16[2,768,1056]{1,2,0:T(8,128)(2,1)S(1)} convert(f32[2,768,1056]{1,2,0:T(8,128)} %param.14) | non-fusion elementwise | flops 1622016 | bytes 9732096 | tf_op jit(solution)/shard_map/convert.4
  17.9 1.7 copy-done.1
  19.6 1.6 fusion.4
  21.3 0.0 all-reduce.5.cloned.1.call-start
  21.4 3.4 %convert.14 = bf16[2,1056,768]{2,1,0:T(8,128)(2,1)S(1)} convert(f32[2,1056,768]{2,1,0:T(8,128)} %param.18) | non-fusion elementwise | flops 1622016 | bytes 9732096 | tf_op jit(solution)/shard_map/convert.3
  24.8 0.6 fusion.44
  25.4 0.6 fusion.45
  26.0 0.1 fusion.31
  26.1 0.1 fusion.29
  26.2 0.7 fusion.37
  26.9 13.9 %psum.28 = f32[256]{0:T(256)S(1)} all-reduce(f32[256]{0:T(256)S(1)} %bitcast.56), channel_id=1, replica_groups=mesh['ra'=4,'cb'=8] {'ra'}, use_global_device_ids=true, to_apply=%region_2.0 | all-reduce | flops 256 | bytes 2048 | tf_op jit(solution)/shard_map/psum | solution.py:35
  40.8 0.5 add_rsqrt_fusion.1
  41.4 4.3 %reduce-scatter.5.cloned.1.call-done = f32[256,264]{0,1:T(8,128)} async-done(((f32[256,1056]{0,1:T(8,128)}), f32[256,264]{0,1:T(8,128)}) %reduce-scatter.5.cloned.1.call-update) | async-done | bytes 270352 | tf_op jit(solution)/shard_map/reduce_scatter | solution.py:32
  45.7 28.7 %reduce-scatter.7.cloned.1.call-done = f32[256,264]{0,1:T(8,128)} async-done(((f32[256,1056]{0,1:T(8,128)}), f32[256,264]{0,1:T(8,128)}) %reduce-scatter.7.cloned.1.call-update) | async-done | bytes 270352 | tf_op jit(solution)/shard_map/reduce_scatter | solution.py:33
  74.3 1.9 multiply_multiply_fusion.3
  76.2 1.8 reshape.75
  78.0 0.8 reshape.76
  78.8 3.7 %fusion.28 = bf16[2,128,264]{1,0,2:T(2,128)(2,1)S(1)} fusion(f32[2,128,264]{1,0,2:T(2,128)} %reshape.76, f32[2,128,264]{1,0,2:T(2,128)} %reshape.75, f32[264]{0:T(512)} %get-tuple-element.10, f32[264]{0:T(512)S(1)} %get-tuple-element.9, f32[264]{0:T(512)S(1)} %get-tuple-element.8, f32[264]{0:T(512)S(1)} %get-tuple-element.32), kind=kLoop, calls=%fused_computation.49 | loop fusion | flops 811008 | bytes 680064 | tf_op jit(solution)/shard_map/convert_element_type | solution.py:47
  82.6 16.0 %all_gather.6 = bf16[256,1056]{0,1:T(8,128)(2,1)S(1)} all-gather(bf16[256,264]{0,1:T(8,128)(2,1)S(1)} %bitcast.54), channel_id=1, replica_groups=mesh['ra'=4,'cb'=8] {'ra'}, dimensions={1}, use_global_device_ids=true | all-gather | bytes 675840 | tf_op jit(solution)/shard_map/all_gather | solution.py:51
  98.6 1.6 fusion.3
  100.2 0.0 reduce-scatter.11.cloned.1.call-start
  100.3 54.1 %all-reduce.5.cloned.1.call-done = f32[256,768]{1,0:T(8,128)} async-done(((f32[256,768]{1,0:T(8,128)}), f32[256,768]{1,0:T(8,128)}) %all-reduce.5.cloned.1.call-update) | async-done | bytes 786448 | tf_op jit(solution)/shard_map/psum | solution.py:53
  154.4 1.6 fusion.11
  156.0 0.7 copy-done.2
  156.7 3.1 %fusion.1 = f32[256,1056]{0,1:T(8,128)} fusion(bf16[2,768,1056]{1,2,0:T(8,128)(2,1)} %copy-done.1, bf16[256,768]{1,0:T(8,128)(2,1)S(1)} %get-tuple-element.16, f32[768]{0:T(1024)S(1)} %copy-done.9), kind=kOutput, calls=%fused_computation.3 | convolution fusion | flops 415825920 | bytes 3099648 | tf_op jit(solution)/shard_map/dot_general | solution.py:30
  159.8 0.0 reduce-scatter.9.cloned.1.call-start
  159.9 3.2 %fusion.2 = f32[256,1056]{0,1:T(8,128)} fusion(bf16[2,768,1056]{1,2,0:T(8,128)(2,1)} %copy-done, bf16[256,768]{1,0:T(8,128)(2,1)} %copy-done.2, f32[768]{0:T(1024)S(1)} %copy-done.9), kind=kOutput, calls=%fused_computation.5 | convolution fusion | flops 415825920 | bytes 3099648 | tf_op jit(solution)/shard_map/dot_general | solution.py:29
  163.1 0.0 all-reduce.7.cloned.1.call-start
  163.1 1.4 fusion.35
  164.5 0.1 fusion.39
  164.6 12.2 %psum.30 = f32[256]{0:T(256)S(1)} all-reduce(f32[256]{0:T(256)S(1)} %get-tuple-element.15), channel_id=1, replica_groups=mesh['ra'=4,'cb'=8] {'ra'}, use_global_device_ids=true, to_apply=%region_7.8 | all-reduce | flops 256 | bytes 2048 | tf_op jit(solution)/shard_map/psum | solution.py:35
  176.8 10.4 %reduce-scatter.11.cloned.1.call-done = f32[256,264]{0,1:T(8,128)} async-done(((f32[256,1056]{0,1:T(8,128)}), f32[256,264]{0,1:T(8,128)}) %reduce-scatter.11.cloned.1.call-update) | async-done | bytes 270352 | tf_op jit(solution)/shard_map/reduce_scatter | solution.py:33
  187.2 28.5 %reduce-scatter.9.cloned.1.call-done = f32[256,264]{0,1:T(8,128)} async-done(((f32[256,1056]{0,1:T(8,128)}), f32[256,264]{0,1:T(8,128)}) %reduce-scatter.9.cloned.1.call-update) | async-done | bytes 270352 | tf_op jit(solution)/shard_map/reduce_scatter | solution.py:32
  215.8 1.9 multiply_multiply_fusion.1
  217.6 1.8 reshape.78
  219.4 0.8 reshape.79
  220.3 3.7 %fusion.27 = bf16[2,128,264]{1,0,2:T(2,128)(2,1)S(1)} fusion(f32[2,128,264]{1,0,2:T(2,128)} %reshape.79, f32[2,128,264]{1,0,2:T(2,128)} %reshape.78, f32[264]{0:T(512)S(1)} %get-tuple-element.7, f32[264]{0:T(512)S(1)} %get-tuple-element.6, f32[264]{0:T(512)S(1)} %get-tuple-element.5, f32[264]{0:T(512)S(1)} %get-tuple-element.33), kind=kLoop, calls=%fused_computation.48 | loop fusion | flops 811008 | bytes 680064 | tf_op jit(solution)/shard_map/convert_element_type | solution.py:47
  224.0 16.0 %all_gather.7 = bf16[256,1056]{0,1:T(8,128)(2,1)S(1)} all-gather(bf16[256,264]{0,1:T(8,128)(2,1)S(1)} %bitcast.55), channel_id=1, replica_groups=mesh['ra'=4,'cb'=8] {'ra'}, dimensions={1}, use_global_device_ids=true | all-gather | bytes 675840 | tf_op jit(solution)/shard_map/all_gather | solution.py:51
  240.0 1.6 fusion
  241.6 54.3 %all-reduce.7.cloned.1.call-done = f32[256,768]{1,0:T(8,128)} async-done(((f32[256,768]{1,0:T(8,128)}), f32[256,768]{1,0:T(8,128)}) %all-reduce.7.cloned.1.call-update) | async-done | bytes 786448 | tf_op jit(solution)/shard_map/psum | solution.py:53
  295.9 2.1 fusion.9
  (29 shorter events, 0.2 us)
Async XLA Ops:
  6.5 39.1 %reduce-scatter.5.cloned.1.call-start = ((), (), s32[]{:S(2)}) async-start(), calls=%async_computation.4 | async-start | bytes 1351680 | tf_op jit(solution)/shard_map/reduce_scatter | solution.py:32
  7.9 3.2 %copy-start.3 = (bf16[2,128,768]{2,1,0:T(8,128)(2,1)S(1)}, bf16[2,128,768]{2,1,0:T(8,128)(2,1)}, u32[]{:S(2)}) copy-start(bf16[2,128,768]{2,1,0:T(8,128)(2,1)} %param.10) | copy-start | bytes 1179652
  11.1 1.9 copy-start
  14.7 59.6 %reduce-scatter.7.cloned.1.call-start = ((), (), s32[]{:S(2)}) async-start(), calls=%async_computation.5 | async-start | bytes 1351680 | tf_op jit(solution)/shard_map/reduce_scatter | solution.py:33
  17.9 1.7 copy-start.1
  21.3 133.1 %all-reduce.5.cloned.1.call-start = ((), (), s32[]{:S(2)}) async-start(), calls=%async_computation.6 | async-start | bytes 1572864 | tf_op jit(solution)/shard_map/psum | solution.py:53
  21.4 3.4 %copy-start.5 = (f32[2,1056]{1,0:T(2,128)S(1)}, f32[2,1056]{1,0:T(2,128)}, u32[]{:S(2)}) copy-start(f32[2,1056]{1,0:T(2,128)} %param.13) | copy-start | bytes 25348
  21.4 4.0 %copy-start.6 = (f32[2,1056]{1,0:T(2,128)S(1)}, f32[2,1056]{1,0:T(2,128)}, u32[]{:S(2)}) copy-start(f32[2,1056]{1,0:T(2,128)} %param.15) | copy-start | bytes 25348
  21.4 4.7 %copy-start.7 = (f32[2,1056]{1,0:T(2,128)S(1)}, f32[2,1056]{1,0:T(2,128)}, u32[]{:S(2)}) copy-start(f32[2,1056]{1,0:T(2,128)} %param.17) | copy-start | bytes 25348
  21.4 4.8 %copy-start.4 = (f32[2,3,1056]{2,0,1:T(2,128)S(1)}, f32[2,3,1056]{2,0,1:T(2,128)}, u32[]{:S(2)}) copy-start(f32[2,3,1056]{2,0,1:T(2,128)} %param.16) | copy-start | bytes 76036
  98.6 1.7 copy-start.8
  100.2 56.5 %copy-start.9 = (f32[768]{0:T(1024)S(1)}, f32[768]{0:T(1024)}, u32[]{:S(2)}) copy-start(f32[768]{0:T(1024)} %get-tuple-element.13) | copy-start | bytes 9220
  100.2 87.0 %reduce-scatter.11.cloned.1.call-start = ((), (), s32[]{:S(2)}) async-start(), calls=%async_computation.8 | async-start | bytes 1351680 | tf_op jit(solution)/shard_map/reduce_scatter | solution.py:33
  156.0 0.7 copy-start.2
  159.8 56.0 %reduce-scatter.9.cloned.1.call-start = ((), (), s32[]{:S(2)}) async-start(), calls=%async_computation.7 | async-start | bytes 1351680 | tf_op jit(solution)/shard_map/reduce_scatter | solution.py:32
  163.1 132.8 %all-reduce.7.cloned.1.call-start = ((), (), s32[]{:S(2)}) async-start(), calls=%async_computation.9 | async-start | bytes 1572864 | tf_op jit(solution)/shard_map/psum | solution.py:53
Sparse Core Ops, SparseCore 0:
  14.8 30.7 reduce-scatter.4
  48.0 26.3 reduce-scatter.6
  100.4 53.9 all-reduce.4
  159.9 27.2 reduce-scatter.10
  189.4 26.3 reduce-scatter.8
  241.8 54.0 all-reduce.6
where the time goes:
time: 306 us; the launch traced here: 305 us
  waiting for transfers between devices  180 us (59%)
  blocking collectives  58.2 us (19%)
  other arithmetic  26.3 us (9%)
  between operations  13.7 us (4%)
  local copies, waits for them, and re-layouts  13.4 us (4%)
  matrix products  12.7 us (4%)
    psum x2, waiting for transfers between devices, sublayer(): down_sum = lax.psum(down_part, 'cb')  108 us
    reduce_scatter x2, waiting for transfers between devices, sublayer(): lax.psum_scatter(up_part, 'ra', scatter_dimension=1, tiled=True)  39.1 us
    reduce_scatter x2, waiting for transfers between devices, sublayer(): lax.psum_scatter(gate_part, 'ra', scatter_dimension=1, tiled=True)  32.8 us
    all_gather x2, blocking collectives, sublayer(): hidden_act = lax.all_gather(hidden_act, 'ra', axis=1, tiled=True)  32 us
    psum x2, blocking collectives, sublayer(): square_sum = lax.psum(squares, 'ra')  26.1 us
    another operation x3, other arithmetic  9.73 us
    convert_element_type x2, other arithmetic, sublayer(): (jax.nn.silu(conv_out) * up_sum.reshape(sequences, length, units)).astype...  7.42 us
  transfers between devices with their start and end apart: 6, of which 6 were waited for; matrix products, arithmetic and copies ran while one was open for 5% of the time, Pallas kernels for 0%

commit v1 on v0

--- a/solution.py
+++ b/solution.py
@@ -50,7 +50,8 @@
     hidden_act = hidden_act.reshape(row_count, units)
     hidden_act = lax.all_gather(hidden_act, "ra", axis=1, tiled=True)
     down_part = jnp.dot(hidden_act, down_w.astype(jnp.bfloat16), preferred_element_type=jnp.float32)
-    down_sum = lax.psum(down_part, "cb")
+    parts = lax.all_gather(down_part, "cb", axis=0, tiled=False)
+    down_sum = parts.sum(axis=0)
     branch = down_sum * down_s[None, :]
     return (
         (residual_keep * values + branch)

time: 306 us -> 292 us (0.954)
  waiting for transfers between devices: 180 us -> 161 us
  other arithmetic: 26.3 us -> 31.6 us
    psum x2 -> x0, waiting for transfers between devices: 108 us -> none  [sublayer(): down_sum = lax.psum(down_part, 'cb')]
    all_gather x0 -> x2, waiting for transfers between devices: none -> 87.9 us  [sublayer(): parts = lax.all_gather(down_part, 'cb', axis=0, tiled=False)]
    reduce_scatter x2, waiting for transfers between devices: 39.1 us -> 57.1 us  [sublayer(): lax.psum_scatter(up_part, 'ra', scatter_dimension=1, tiled=True)]
    reduce_scatter x2, waiting for transfers between devices: 32.8 us -> 15.5 us  [sublayer(): lax.psum_scatter(gate_part, 'ra', scatter_dimension=1, tiled=True)]
    reduce_sum x0 -> x2, other arithmetic: none -> 7.46 us  [sublayer(): down_sum = parts.sum(axis=0)]
where the time goes in v1:
time: 292 us; the launch traced here: 291 us
  waiting for transfers between devices  161 us (55%)
  blocking collectives  58.1 us (20%)
  other arithmetic  31.6 us (11%)
  local copies, waits for them, and re-layouts  13.8 us (5%)
  between operations  13.7 us (5%)
  matrix products  12.8 us (4%)
    all_gather x2, waiting for transfers between devices, sublayer(): parts = lax.all_gather(down_part, 'cb', axis=0, tiled=False)  87.9 us
    reduce_scatter x2, waiting for transfers between devices, sublayer(): lax.psum_scatter(up_part, 'ra', scatter_dimension=1, tiled=True)  57.1 us
    all_gather x2, blocking collectives, sublayer(): hidden_act = lax.all_gather(hidden_act, 'ra', axis=1, tiled=True)  32 us
    psum x2, blocking collectives, sublayer(): square_sum = lax.psum(squares, 'ra')  26.1 us
    reduce_scatter x2, waiting for transfers between devices, sublayer(): lax.psum_scatter(gate_part, 'ra', scatter_dimension=1, tiled=True)  15.5 us
    another operation x3, other arithmetic  9.78 us
    reduce_sum x2, other arithmetic, sublayer(): down_sum = parts.sum(axis=0)  7.46 us
    convert_element_type x2, other arithmetic, sublayer(): (jax.nn.silu(conv_out) * up_sum.reshape(sequences, length, units)).astype...  7.43 us
  transfers between devices with their start and end apart: 6, of which 6 were waited for; matrix products, arithmetic and copies ran while one was open for 5% of the time, Pallas kernels for 0%

profile of v1, /device:TPU:0, one launch (start us, length us, event | category | flops | bytes accessed | tf_op | source)
XLA Modules:
  0.0 290.8 jit_solution(17911828176781684965)
XLA Ops:
  6.5 0.8 slice_reduce_fusion.1
  7.3 3.2 %convert.12 = bf16[2,768,1056]{1,2,0:T(8,128)(2,1)S(1)} convert(f32[2,768,1056]{1,2,0:T(8,128)} %param.12) | non-fusion elementwise | flops 1622016 | bytes 9732096 | tf_op jit(solution)/shard_map/convert.5
  10.6 0.2 fusion.9
  10.8 0.9 copy-done.2
  11.7 1.6 fusion.5
  13.4 3.2 %convert.13 = bf16[2,768,1056]{1,2,0:T(8,128)(2,1)S(1)} convert(f32[2,768,1056]{1,2,0:T(8,128)} %param.14) | non-fusion elementwise | flops 1622016 | bytes 9732096 | tf_op jit(solution)/shard_map/convert.4
  16.6 1.7 copy-done.1
  18.3 1.6 fusion.4
  20.0 0.0 all-gather.5.cloned.1.call-start
  20.1 3.4 %convert.14 = bf16[2,1056,768]{2,1,0:T(8,128)(2,1)S(1)} convert(f32[2,1056,768]{2,1,0:T(8,128)} %param.18) | non-fusion elementwise | flops 1622016 | bytes 9732096 | tf_op jit(solution)/shard_map/convert.3
  23.5 0.6 fusion.43
  24.1 0.6 fusion.44
  24.7 0.1 fusion.30
  24.8 0.1 fusion.28
  24.9 0.7 fusion.36
  25.6 13.9 %psum.14 = f32[256]{0:T(256)S(1)} all-reduce(f32[256]{0:T(256)S(1)} %bitcast.64), channel_id=1, replica_groups=mesh['ra'=4,'cb'=8] {'ra'}, use_global_device_ids=true, to_apply=%region_2.0 | all-reduce | flops 256 | bytes 2048 | tf_op jit(solution)/shard_map/psum | solution.py:35
  39.5 0.6 add_rsqrt_fusion.1
  40.0 4.3 %reduce-scatter.5.cloned.1.call-done = f32[256,264]{0,1:T(8,128)} async-done(((f32[256,1056]{0,1:T(8,128)}), f32[256,264]{0,1:T(8,128)}) %reduce-scatter.5.cloned.1.call-update) | async-done | bytes 270352 | tf_op jit(solution)/shard_map/reduce_scatter | solution.py:32
  44.3 28.7 %reduce-scatter.7.cloned.1.call-done = f32[256,264]{0,1:T(8,128)} async-done(((f32[256,1056]{0,1:T(8,128)}), f32[256,264]{0,1:T(8,128)}) %reduce-scatter.7.cloned.1.call-update) | async-done | bytes 270352 | tf_op jit(solution)/shard_map/reduce_scatter | solution.py:33
  73.0 1.9 multiply_multiply_fusion.3
  74.8 1.8 reshape.96
  76.6 0.8 reshape.97
  77.5 3.7 %fusion.27 = bf16[2,128,264]{1,0,2:T(2,128)(2,1)S(1)} fusion(f32[2,128,264]{1,0,2:T(2,128)} %reshape.97, f32[2,128,264]{1,0,2:T(2,128)} %reshape.96, f32[264]{0:T(512)} %get-tuple-element.10, f32[264]{0:T(512)} %get-tuple-element.9, f32[264]{0:T(512)S(1)} %get-tuple-element.8, f32[264]{0:T(512)S(1)} %get-tuple-element.31), kind=kLoop, calls=%fused_computation.49 | loop fusion | flops 811008 | bytes 680064 | tf_op jit(solution)/shard_map/convert_element_type | solution.py:47
  81.3 16.0 %all_gather.18 = bf16[256,1056]{0,1:T(8,128)(2,1)S(1)} all-gather(bf16[256,264]{0,1:T(8,128)(2,1)S(1)} %bitcast.62), channel_id=1, replica_groups=mesh['ra'=4,'cb'=8] {'ra'}, dimensions={1}, use_global_device_ids=true | all-gather | bytes 675840 | tf_op jit(solution)/shard_map/all_gather | solution.py:51
  97.3 1.7 fusion.3
  99.1 43.9 %all-gather.5.cloned.1.call-done = f32[2048,768]{1,0:T(8,128)} async-done(((f32[256,768]{1,0:T(8,128)}), f32[2048,768]{1,0:T(8,128)}) %all-gather.5.cloned.1.call-update) | async-done | bytes 6291472 | tf_op jit(solution)/shard_map/all_gather | solution.py:53
  142.9 4.2 %reduce_sum.46 = f32[256,768]{1,0:T(8,128)} reduce(f32[8,256,768]{2,1,0:T(8,128)} %bitcast.52, f32[]{:T(128)} %constant.30.clone.1), dimensions={0}, to_apply=%region_4.5 | reduce | flops 1376256 | bytes 7077892 | tf_op jit(solution)/shard_map/reduce_sum | solution.py:54
  147.1 1.5 fusion.13
  148.6 0.7 copy-done.5
  149.3 0.1 fusion.12
  149.4 0.7 copy-done.4
  150.2 3.0 %fusion.2 = f32[256,1056]{0,1:T(8,128)} fusion(bf16[256,768]{1,0:T(8,128)(2,1)S(1)} %bitcast.56, bf16[2,768,1056]{1,2,0:T(8,128)(2,1)} %copy-done), kind=kOutput, calls=%fused_computation.5 | convolution fusion | flops 415236096 | bytes 3096576 | tf_op jit(solution)/shard_map/dot_general | solution.py:29
  153.3 3.2 %fusion.1 = f32[256,1056]{0,1:T(8,128)} fusion(bf16[256,768]{1,0:T(8,128)(2,1)} %bitcast.57, bf16[2,768,1056]{1,2,0:T(8,128)(2,1)} %copy-done.1), kind=kOutput, calls=%fused_computation.3 | convolution fusion | flops 415236096 | bytes 3096576 | tf_op jit(solution)/shard_map/dot_general | solution.py:30
  156.5 0.0 all-gather.7.cloned.1.call-start
  156.6 1.4 fusion.34
  157.9 0.1 fusion.38
  158.0 12.2 %psum.15 = f32[256]{0:T(256)S(1)} all-reduce(f32[256]{0:T(256)S(1)} %bitcast.65), channel_id=1, replica_groups=mesh['ra'=4,'cb'=8] {'ra'}, use_global_device_ids=true, to_apply=%region_7.8 | all-reduce | flops 256 | bytes 2048 | tf_op jit(solution)/shard_map/psum | solution.py:35
  170.2 11.2 %reduce-scatter.9.cloned.1.call-done = f32[256,264]{0,1:T(8,128)} async-done(((f32[256,1056]{0,1:T(8,128)}), f32[256,264]{0,1:T(8,128)}) %reduce-scatter.9.cloned.1.call-update) | async-done | bytes 270352 | tf_op jit(solution)/shard_map/reduce_scatter | solution.py:32
  181.4 28.5 %reduce-scatter.11.cloned.1.call-done = f32[256,264]{0,1:T(8,128)} async-done(((f32[256,1056]{0,1:T(8,128)}), f32[256,264]{0,1:T(8,128)}) %reduce-scatter.11.cloned.1.call-update) | async-done | bytes 270352 | tf_op jit(solution)/shard_map/reduce_scatter | solution.py:33
  209.9 1.9 multiply_multiply_fusion.1
  211.8 1.8 reshape.99
  213.6 0.8 reshape.100
  214.4 3.7 %fusion.26 = bf16[2,128,264]{1,0,2:T(2,128)(2,1)S(1)} fusion(f32[2,128,264]{1,0,2:T(2,128)} %reshape.100, f32[2,128,264]{1,0,2:T(2,128)} %reshape.99, f32[264]{0:T(512)S(1)} %get-tuple-element.7, f32[264]{0:T(512)S(1)} %get-tuple-element.6, f32[264]{0:T(512)S(1)} %get-tuple-element.5, f32[264]{0:T(512)S(1)} %get-tuple-element.32), kind=kLoop, calls=%fused_computation.48 | loop fusion | flops 811008 | bytes 680064 | tf_op jit(solution)/shard_map/convert_element_type | solution.py:47
  218.1 16.0 %all_gather.21 = bf16[256,1056]{0,1:T(8,128)(2,1)S(1)} all-gather(bf16[256,264]{0,1:T(8,128)(2,1)S(1)} %bitcast.63), channel_id=1, replica_groups=mesh['ra'=4,'cb'=8] {'ra'}, dimensions={1}, use_global_device_ids=true | all-gather | bytes 675840 | tf_op jit(solution)/shard_map/all_gather | solution.py:51
  234.2 1.6 fusion
  235.8 44.0 %all-gather.7.cloned.1.call-done = f32[2048,768]{1,0:T(8,128)} async-done(((f32[256,768]{1,0:T(8,128)}), f32[2048,768]{1,0:T(8,128)}) %all-gather.7.cloned.1.call-update) | async-done | bytes 6291472 | tf_op jit(solution)/shard_map/all_gather | solution.py:53
  279.8 3.3 %reduce_sum.50 = f32[256,768]{1,0:T(8,128)S(1)} reduce(f32[8,256,768]{2,1,0:T(8,128)} %bitcast.53, f32[]{:T(128)} %constant.30.clone.1), dimensions={0}, to_apply=%region_9.10 | reduce | flops 1376256 | bytes 7077892 | tf_op jit(solution)/shard_map/reduce_sum | solution.py:54
  283.0 0.9 fusion.11
  (38 shorter events, 0.4 us)
Async XLA Ops:
  6.5 37.8 %reduce-scatter.5.cloned.1.call-start = ((), (), s32[]{:S(2)}) async-start(), calls=%async_computation.4 | async-start | bytes 1351680 | tf_op jit(solution)/shard_map/reduce_scatter | solution.py:32
  7.3 3.2 %copy-start.7 = (bf16[2,128,768]{2,1,0:T(8,128)(2,1)S(1)}, bf16[2,128,768]{2,1,0:T(8,128)(2,1)}, u32[]{:S(2)}) copy-start(bf16[2,128,768]{2,1,0:T(8,128)(2,1)} %param.10) | copy-start | bytes 1179652
  10.6 9.5 %copy-start = (bf16[2,768,1056]{1,2,0:T(8,128)(2,1)}, bf16[2,768,1056]{1,2,0:T(8,128)(2,1)S(1)}, u32[]{:S(2)}) copy-start(bf16[2,768,1056]{1,2,0:T(8,128)(2,1)S(1)} %convert.12) | copy-start | bytes 9732100
  10.8 1.0 copy-start.2
  13.4 59.6 %reduce-scatter.7.cloned.1.call-start = ((), (), s32[]{:S(2)}) async-start(), calls=%async_computation.5 | async-start | bytes 1351680 | tf_op jit(solution)/shard_map/reduce_scatter | solution.py:33
  13.4 4.9 %copy-start.3 = (bf16[2,128,768]{2,1,0:T(8,128)(2,1)S(1)}, bf16[2,128,768]{2,1,0:T(8,128)(2,1)}, u32[]{:S(2)}) copy-start(bf16[2,128,768]{2,1,0:T(8,128)(2,1)} %copy-done.2) | copy-start | bytes 1179652
  16.6 1.7 copy-start.1
  20.0 123.0 %all-gather.5.cloned.1.call-start = ((), (), s32[]{:S(2)}) async-start(), calls=%async_computation.8 | async-start | bytes 7077888 | tf_op jit(solution)/shard_map/all_gather | solution.py:53
  20.0 3.4 %copy-start.9 = (f32[2,1056]{1,0:T(2,128)S(1)}, f32[2,1056]{1,0:T(2,128)}, u32[]{:S(2)}) copy-start(f32[2,1056]{1,0:T(2,128)} %param.13) | copy-start | bytes 25348
  20.1 4.0 %copy-start.10 = (f32[2,1056]{1,0:T(2,128)S(1)}, f32[2,1056]{1,0:T(2,128)}, u32[]{:S(2)}) copy-start(f32[2,1056]{1,0:T(2,128)} %param.15) | copy-start | bytes 25348
  20.1 4.7 %copy-start.11 = (f32[2,1056]{1,0:T(2,128)S(1)}, f32[2,1056]{1,0:T(2,128)}, u32[]{:S(2)}) copy-start(f32[2,1056]{1,0:T(2,128)} %param.17) | copy-start | bytes 25348
  20.1 4.8 %copy-start.8 = (f32[2,3,1056]{2,0,1:T(2,128)S(1)}, f32[2,3,1056]{2,0,1:T(2,128)}, u32[]{:S(2)}) copy-start(f32[2,3,1056]{2,0,1:T(2,128)} %param.16) | copy-start | bytes 76036
  74.8 24.2 %copy-start.12 = (f32[2,768]{1,0:T(2,128)S(1)}, f32[2,768]{1,0:T(2,128)}, u32[]{:S(2)}) copy-start(f32[2,768]{1,0:T(2,128)} %param.19) | copy-start | bytes 18436
  99.0 82.5 %reduce-scatter.9.cloned.1.call-start = ((), (), s32[]{:S(2)}) async-start(), calls=%async_computation.6 | async-start | bytes 1351680 | tf_op jit(solution)/shard_map/reduce_scatter | solution.py:32
  148.6 0.7 copy-start.5
  149.4 0.7 copy-start.4
  153.2 56.7 %reduce-scatter.11.cloned.1.call-start = ((), (), s32[]{:S(2)}) async-start(), calls=%async_computation.7 | async-start | bytes 1351680 | tf_op jit(solution)/shard_map/reduce_scatter | solution.py:33
  156.5 123.2 %all-gather.7.cloned.1.call-start = ((), (), s32[]{:S(2)}) async-start(), calls=%async_computation.9 | async-start | bytes 7077888 | tf_op jit(solution)/shard_map/all_gather | solution.py:53
  279.7 3.3 %copy-start.6 = (bf16[2,128,768]{2,1,0:T(8,128)(2,1)S(1)}, bf16[2,128,768]{2,1,0:T(8,128)(2,1)}, u32[]{:S(2)}) copy-start(bf16[2,128,768]{2,1,0:T(8,128)(2,1)} %copy-done.5) | copy-start | bytes 1179652
Sparse Core Ops, SparseCore 0:
  13.5 30.7 reduce-scatter.4
  46.6 26.3 reduce-scatter.6
  99.1 43.8 all-gather.4
  153.3 28.0 reduce-scatter.8
  183.6 26.2 reduce-scatter.10
  235.9 43.8 all-gather.6
